TPU v7x, 32 devices: a whole 2x2x4 slice. The times are simulated.
32 devices in a mesh: kv: 8 (over z, x), tp: 4 (over y, core).
Axes of the slice: x: 2, y: 2, z: 4, core: 2. Of those that a mesh axis runs over, the one named last changes fastest.
Arguments:
- tokens: bfloat16 [128, 2048], P(None, 'kv'), may hold values from -16 to 16
- norm_gain: bfloat16 [2048], P('kv'), may hold values from 0.099609375 to 1.8984375
- w_query: bfloat16 [2048, 1024], P('kv', 'tp'), may hold values from -0.125 to 0.125
- w_key: bfloat16 [2048, 1024], P('kv', 'tp'), may hold values from -0.125 to 0.125
- w_value: bfloat16 [2048, 2048], P('kv', 'tp'), may hold values from -0.125 to 0.125
- w_gate: bfloat16 [2048, 2048], P('kv', 'tp'), may hold values from -0.125 to 0.125
- w_decay: bfloat16 [2048, 1024], P('kv', 'tp'), may hold values from -0.5 to 0.5
- log_decay: float32 [128, 1024], P('kv', 'tp'), may hold values from -1.5 to 0
- state: float32 [128, 8, 128, 256], P('kv', 'tp'), may hold values from -6 to 6
- out_gain: float32 [256], replicated, may hold values from 0.1 to 1.9
- w_out: bfloat16 [2048, 2048], P('tp', 'kv'), may hold values from -0.125 to 0.125
- mixer_gain: bfloat16 [2048], P('kv'), may hold values from 0.099609375 to 1.8984375
- w_ffgate: bfloat16 [2048, 6144], P('kv', 'tp'), may hold values from -0.125 to 0.125
- w_ffup: bfloat16 [2048, 6144], P('kv', 'tp'), may hold values from -0.125 to 0.125
- w_down: bfloat16 [6144, 2048], P('tp', 'kv'), may hold values from -0.078125 to 0.078125
Outputs:
- result: bfloat16 [128, 2048], P(None, 'kv')
- new_state: float32 [128, 8, 128, 256], P('kv', 'tp')
All inputs are finite; a program needn't handle non-finite values.
Results may differ from a plain program's by a relative error of at most 0.028.
Values may be sent and summed in bfloat16 or wider, within the bound.
A program may use at most 64 MiB of HBM per device.

v0:
```python
import functools

import jax
import jax.numpy as jnp
from jax import lax
from jax.experimental import pallas as pl
from jax.experimental.pallas import tpu as pltpu
from jax.sharding import PartitionSpec as P

eps = 1e-06
gate_norm = 16.0
LANES = 128
CHUNKS = 6
LAG_Z = 6
LAG_X = 8
F32 = jnp.float32
BF16 = jnp.bfloat16


def remote(src, dst, send_sem, recv_sem, device):
    return pltpu.make_async_remote_copy(
        src_ref=src,
        dst_ref=dst,
        send_sem=send_sem,
        recv_sem=recv_sem,
        device_id=device,
        device_id_type=pl.DeviceIdType.MESH,
    )


def split_axis(n_kv):
    n_in = 1
    while n_in * n_in * 4 <= n_kv:
        n_in *= 2
    return n_kv // n_in, n_in


def ff_chunks(width):
    if width % LANES:
        return [(0, width)]
    left, at, ranges = width // LANES, 0, []
    while left:
        take = min(left, -(-(width // LANES) // CHUNKS))
        ranges.append((at, at + take * LANES))
        at += take * LANES
        left -= take
    return ranges


def kernel(
    n_kv,
    n_tp,
    d_model,
    tokens_ref,
    norm_gain_ref,
    wq_hbm,
    wk_hbm,
    wv_hbm,
    wg_hbm,
    wd_hbm,
    log_decay_ref,
    state_hbm,
    out_gain_ref,
    wo_hbm,
    mixer_gain_ref,
    wfg_hbm,
    wfu_hbm,
    wdn_hbm,
    result_ref,
    ns_ref,
    wq,
    wk,
    wv,
    wg,
    wd,
    wo,
    wfg,
    wfu,
    wdn,
    px,
    rx,
    pz,
    rz,
    att,
    mg,
    to,
    fx,
    frx,
    fz,
    frz,
    hg,
    td,
    middle_ref,
    load_sem,
    ax_s,
    ax_r,
    az_s,
    az_r,
    mz_s,
    mz_r,
    mx_s,
    mx_r,
    to_s,
    to_r,
    fx_s,
    fx_r,
    fz_s,
    fz_r,
    hz_s,
    hz_r,
    hx_s,
    hx_r,
    td_s,
    td_r,
):
    n_out, n_in = split_axis(n_kv)
    kv = lax.axis_index("kv")
    tp = lax.axis_index("tp")
    zi = kv // n_in
    xi = lax.rem(kv, n_in)
    rows = px.shape[2]
    batch = tokens_ref.shape[0]

    def x_peer(d):
        return lax.rem(xi + d, n_in)

    def z_peer(d):
        return lax.rem(zi + d, n_out)

    def z_back(d):
        return lax.rem(zi + n_out - d, n_out)

    def x_back(d):
        return lax.rem(xi + n_in - d, n_in)

    def x_dev(d):
        return (zi * n_in + x_peer(d), tp)

    def z_dev(d):
        return (z_peer(d) * n_in + xi, tp)

    def t_dev(d):
        return (kv, lax.rem(tp + d, n_tp))

    barrier = pltpu.get_barrier_semaphore()
    peers = (
        [x_dev(d) for d in range(1, n_in)]
        + [z_dev(d) for d in range(1, n_out)]
        + [t_dev(d) for d in range(1, n_tp)]
    )
    for dev in peers:
        pl.semaphore_signal(barrier, inc=1, device_id=dev, device_id_type=pl.DeviceIdType.MESH)

    loads = [
        pltpu.make_async_copy(src, dst, load_sem.at[i])
        for i, (src, dst) in enumerate(
            (
                (wq_hbm, wq),
                (wk_hbm, wk),
                (wd_hbm, wd),
                (wv_hbm, wv),
                (wg_hbm, wg),
                (state_hbm, ns_ref),
                (wo_hbm, wo),
                (wfg_hbm, wfg),
                (wfu_hbm, wfu),
                (wdn_hbm, wdn),
            )
        )
    ]
    for load in loads[:5]:
        load.start()
    load_q, load_k, load_d, load_v, load_g, load_state, load_o, load_fg, load_fu, load_dn = loads

    pending = []

    def launch(copy):
        copy.start()
        pending.append(copy)

    def scatter_rows(dst, value, lo):
        width = value.shape[1]
        value = value.astype(BF16)
        for z in range(n_out):
            for x in range(n_in):
                at = (z * n_in + x) * rows
                dst[x, z, :, lo : lo + width] = value[at : at + rows]

    def send_x(src, dst, s, r, c, lo, hi):
        cols = slice(lo, hi)
        return [
            remote(
                src.at[x_peer(d), :, :, cols],
                dst.at[d - 1, :, :, cols],
                s.at[c, d - 1],
                r.at[c, d - 1],
                x_dev(d),
            )
            for d in range(1, n_in)
        ]

    def send_z(src, dst, s, r, c, lo, hi):
        cols = slice(lo, hi)
        return [
            remote(
                src.at[z_peer(d), :, cols],
                dst.at[d - 1, :, cols],
                s.at[c, d - 1],
                r.at[c, d - 1],
                z_dev(d),
            )
            for d in range(1, n_out)
        ]

    def reduce_x(src, got, dst, copies, lo, hi):
        for copy in copies:
            copy.wait_recv()
        total = src[xi, :, :, lo:hi].astype(F32)
        for d in range(1, n_in):
            total = total + got[d - 1, :, :, lo:hi].astype(F32)
        dst[:, :, lo:hi] = total.astype(BF16)

    def reduce_z(src, got, copies, lo, hi):
        for copy in copies:
            copy.wait_recv()
        total = src[zi, :, lo:hi].astype(F32)
        for d in range(1, n_out):
            total = total + got[d - 1, :, lo:hi].astype(F32)
        return total

    wide = tokens_ref[...].astype(F32)
    scaled = (wide * norm_gain_ref[...].astype(F32).reshape(1, -1)).astype(BF16)
    squares = jnp.broadcast_to(jnp.sum(wide * wide, axis=1, keepdims=True), (batch, LANES))

    kw = wq.shape[1]
    vw = wv.shape[1]
    q_at = LANES
    k_at = q_at + kw
    d_at = k_at + kw
    v_at = d_at + kw
    g_at = v_at + vw
    end = g_at + vw
    bounds = ((0, d_at), (d_at, g_at), (g_at, end))
    parts = (
        ((wq, load_q, q_at), (wk, load_k, k_at)),
        ((wd, load_d, d_at), (wv, load_v, v_at)),
        ((wg, load_g, g_at),),
    )
    x_copies = []
    for c, ((lo, hi), part) in enumerate(zip(bounds, parts)):
        if c == 0:
            scatter_rows(px, squares, 0)
        for weight, load, at in part:
            load.wait()
            scatter_rows(px, jnp.dot(scaled, weight[...], preferred_element_type=F32), at)
        if c == 0:
            pl.semaphore_wait(barrier, len(peers))
        copies = send_x(px, rx, ax_s, ax_r, c, lo, hi)
        for copy in copies:
            launch(copy)
        x_copies.append(copies)
    for load in loads[5:]:
        load.start()
    z_copies = []
    for c, (lo, hi) in enumerate(bounds):
        reduce_x(px, rx, pz, x_copies[c], lo, hi)
        copies = send_z(pz, rz, az_s, az_r, c, lo, hi)
        for copy in copies:
            launch(copy)
        z_copies.append(copies)

    first = reduce_z(pz, rz, z_copies[0], *bounds[0])
    inv = lax.rsqrt(first[:, :1] / d_model + eps)
    second = reduce_z(pz, rz, z_copies[1], *bounds[1])

    heads, dk, dv = ns_ref.shape[1:]
    query = first[:, q_at : q_at + kw] * inv * dk ** (-0.5)
    keys = first[:, k_at : k_at + kw] * inv
    pre = second[:, :kw] * inv
    values = second[:, kw:] * inv
    log_sig = jnp.minimum(pre, 0.0) - jnp.log1p(jnp.exp(-jnp.abs(pre)))
    decay = jnp.exp(log_sig / gate_norm + log_decay_ref[...])
    load_state.wait()
    for h in range(heads):
        ks = slice(h * dk, (h + 1) * dk)
        q_t = query[:, ks].T
        k_t = keys[:, ks].T
        a_t = decay[:, ks].T
        for b in range(rows):
            col = slice(b, b + 1)
            v_row = values[b : b + 1, h * dv : (h + 1) * dv]
            new = ns_ref[b, h] * a_t[:, col] + k_t[:, col] * v_row
            ns_ref[b, h] = new
            att[h, b : b + 1, :] = jnp.sum(new * q_t[:, col], axis=0, keepdims=True)

    gate = reduce_z(pz, rz, z_copies[2], *bounds[2]) * inv
    for h in range(heads):
        got = att[h]
        normed = (
            got
            * lax.rsqrt(jnp.mean(got * got, axis=1, keepdims=True) + eps)
            * out_gain_ref[...]
        )
        cols = slice(h * dv, (h + 1) * dv)
        mg[zi, xi, :, cols] = (normed * jax.nn.silu(gate[:, cols])).astype(BF16)

    def gather_z(buf, cols, s, r):
        for d in range(1, n_out):
            own = buf.at[zi, xi, :, cols]
            launch(remote(own, own, s.at[d - 1], r.at[d - 1], z_dev(d)))

    def forward_x(buf, cols, zs, zr, s, r):
        for dz in range(n_out):
            slot = buf.at[z_back(dz), xi, :, cols]
            if dz:
                remote(slot, slot, zs.at[dz - 1], zr.at[dz - 1], z_dev(dz)).wait_recv()
            for d in range(1, n_in):
                launch(remote(slot, slot, s.at[dz, d - 1], r.at[dz, d - 1], x_dev(d)))

    def arrive_x(buf, cols, s, r):
        for dz in range(n_out):
            for d in range(1, n_in):
                slot = buf.at[z_back(dz), x_back(d), :, cols]
                remote(slot, slot, s.at[dz, d - 1], r.at[dz, d - 1], x_dev(d)).wait_recv()

    gather_z(mg, slice(0, vw), mz_s, mz_r)
    forward_x(mg, slice(0, vw), mz_s, mz_r, mx_s, mx_r)
    load_o.wait()
    arrive_x(mg, slice(0, vw), mx_s, mx_r)

    def sum_groups(buf, s, r):
        for d in range(1, n_tp):
            launch(remote(buf.at[tp], buf.at[tp], s.at[d - 1], r.at[d - 1], t_dev(d)))
        for d in range(1, n_tp):
            slot = buf.at[lax.rem(tp + n_tp - d, n_tp)]
            remote(slot, slot, s.at[d - 1], r.at[d - 1], t_dev(d)).wait_recv()
        total = buf[0].astype(F32)
        for g in range(1, n_tp):
            total = total + buf[g].astype(F32)
        return total

    mixed = mg[...].reshape(batch, vw)
    to[tp] = jnp.dot(mixed, wo[...], preferred_element_type=F32).astype(BF16)
    middle = (tokens_ref[...].astype(F32) + sum_groups(to, to_s, to_r)).astype(BF16)
    middle_ref[...] = middle

    wide2 = middle.astype(F32)
    scaled2 = (wide2 * mixer_gain_ref[...].astype(F32).reshape(1, -1)).astype(BF16)
    squares2 = jnp.broadcast_to(jnp.sum(wide2 * wide2, axis=1, keepdims=True), (batch, LANES))
    ff = wfg.shape[1]
    chunks = ff_chunks(ff)
    n_c = len(chunks)
    fbounds = [(LANES + 2 * lo if lo else 0, LANES + 2 * hi) for lo, hi in chunks]
    load_fg.wait()
    load_fu.wait()
    fx_copies = []
    for c, (lo, hi) in enumerate(fbounds):
        if c == 0:
            scatter_rows(fx, squares2, 0)
        cols = slice(*chunks[c])
        fc = chunks[c][1] - chunks[c][0]
        at = hi - 2 * fc
        scatter_rows(fx, jnp.dot(scaled2, wfg[:, cols], preferred_element_type=F32), at)
        scatter_rows(fx, jnp.dot(scaled2, wfu[:, cols], preferred_element_type=F32), at + fc)
        copies = send_x(fx, frx, fx_s, fx_r, c, lo, hi)
        for copy in copies:
            launch(copy)
        fx_copies.append(copies)

    fz_copies = [None] * n_c
    inv2 = [None]

    def to_z(c):
        lo, hi = fbounds[c]
        reduce_x(fx, frx, fz, fx_copies[c], lo, hi)
        fz_copies[c] = send_z(fz, frz, fz_s, fz_r, c, lo, hi)
        for copy in fz_copies[c]:
            launch(copy)

    def activate(c):
        terms = reduce_z(fz, frz, fz_copies[c], *fbounds[c])
        if c == 0:
            inv2[0] = lax.rsqrt(terms[:, :1] / d_model + eps)
            terms = terms[:, LANES:]
        terms = terms * inv2[0]
        fc = terms.shape[1] // 2
        cols = slice(*chunks[c])
        hg[zi, xi, :, cols] = (jax.nn.silu(terms[:, :fc]) * terms[:, fc:]).astype(BF16)
        gather_z(hg, cols, hz_s.at[c], hz_r.at[c])

    def hand_on(c):
        forward_x(hg, slice(*chunks[c]), hz_s.at[c], hz_r.at[c], hx_s.at[c], hx_r.at[c])

    for t in range(n_c + LAG_X):
        if t < n_c:
            to_z(t)
        if 0 <= t - LAG_Z < n_c:
            activate(t - LAG_Z)
        if 0 <= t - LAG_X < n_c:
            hand_on(t - LAG_X)

    load_dn.wait()
    down = None
    for c, (lo, hi) in enumerate(chunks):
        arrive_x(hg, slice(*chunks[c]), hx_s.at[c], hx_r.at[c])
        term = jnp.dot(
            hg[:, :, :, lo:hi].reshape(batch, hi - lo),
            wdn[lo:hi, :],
            preferred_element_type=F32,
        )
        down = term if down is None else down + term
    td[tp] = down.astype(BF16)
    total = sum_groups(td, td_s, td_r)
    result_ref[...] = (middle_ref[...].astype(F32) + total).astype(BF16)

    for copy in pending:
        copy.wait_send()


def body(n_kv, n_tp, *args):
    (
        tokens,
        norm_gain,
        w_query,
        w_key,
        w_value,
        w_gate,
        w_decay,
        log_decay,
        state,
        out_gain,
        w_out,
        mixer_gain,
        w_ffgate,
        w_ffup,
        w_down,
    ) = args
    n_out, n_in = split_axis(n_kv)
    batch, feats = tokens.shape
    rows, heads, dk, dv = state.shape
    kw = w_query.shape[1]
    vw = w_value.shape[1]
    ff = w_ffgate.shape[1]
    n_c = len(ff_chunks(ff))
    width = LANES + 3 * kw + 2 * vw
    fwidth = LANES + 2 * ff
    m_in, m_out, m_tp = max(n_in - 1, 1), max(n_out - 1, 1), max(n_tp - 1, 1)
    dma = pltpu.SemaphoreType.DMA
    vmem = pltpu.VMEM
    whole = pl.BlockSpec(memory_space=pltpu.VMEM)
    far = pl.BlockSpec(memory_space=pl.ANY)
    sems = [
        (10,),
        (3, m_in),
        (3, m_in),
        (3, m_out),
        (3, m_out),
        (m_out,),
        (m_out,),
        (n_out, m_in),
        (n_out, m_in),
        (m_tp,),
        (m_tp,),
        (n_c, m_in),
        (n_c, m_in),
        (n_c, m_out),
        (n_c, m_out),
        (n_c, m_out),
        (n_c, m_out),
        (n_c, n_out, m_in),
        (n_c, n_out, m_in),
        (m_tp,),
        (m_tp,),
    ]
    result, new_state = pl.pallas_call(
        functools.partial(kernel, n_kv, n_tp, feats * n_kv),
        out_shape=(
            vmem((batch, feats), BF16),
            vmem(state.shape, F32),
        ),
        in_specs=[
            whole,
            whole,
            far,
            far,
            far,
            far,
            far,
            whole,
            far,
            whole,
            far,
            whole,
            far,
            far,
            far,
        ],
        out_specs=(whole, whole),
        scratch_shapes=[
            vmem(w_query.shape, BF16),
            vmem(w_key.shape, BF16),
            vmem(w_value.shape, BF16),
            vmem(w_gate.shape, BF16),
            vmem(w_decay.shape, BF16),
            vmem(w_out.shape, BF16),
            vmem(w_ffgate.shape, BF16),
            vmem(w_ffup.shape, BF16),
            vmem(w_down.shape, BF16),
            vmem((n_in, n_out, rows, width), BF16),
            vmem((m_in, n_out, rows, width), BF16),
            vmem((n_out, rows, width), BF16),
            vmem((m_out, rows, width), BF16),
            vmem((heads, rows, dv), F32),
            vmem((n_out, n_in, rows, vw), BF16),
            vmem((n_tp, batch, feats), BF16),
            vmem((n_in, n_out, rows, fwidth), BF16),
            vmem((m_in, n_out, rows, fwidth), BF16),
            vmem((n_out, rows, fwidth), BF16),
            vmem((m_out, rows, fwidth), BF16),
            vmem((n_out, n_in, rows, ff), BF16),
            vmem((n_tp, batch, feats), BF16),
            vmem((batch, feats), BF16),
        ]
        + [dma(shape) for shape in sems],
        compiler_params=pltpu.CompilerParams(
            collective_id=0, has_side_effects=True, vmem_limit_bytes=56 * 2**20
        ),
    )(
        tokens,
        norm_gain,
        w_query,
        w_key,
        w_value,
        w_gate,
        w_decay,
        log_decay,
        state,
        out_gain.reshape(1, dv),
        w_out,
        mixer_gain,
        w_ffgate,
        w_ffup,
        w_down,
    )
    return (result, new_state)


def solution(mesh):
    return jax.shard_map(
        functools.partial(body, mesh.shape["kv"], mesh.shape["tp"]),
        mesh=mesh,
        in_specs=(
            P(None, "kv"),
            P("kv"),
            P("kv", "tp"),
            P("kv", "tp"),
            P("kv", "tp"),
            P("kv", "tp"),
            P("kv", "tp"),
            P("kv", "tp"),
            P("kv", "tp", None, None),
            P(),
            P("tp", "kv"),
            P("kv"),
            P("kv", "tp"),
            P("kv", "tp"),
            P("tp", "kv"),
        ),
        out_specs=(P(None, "kv"), P("kv", "tp", None, None)),
        check_vma=False,
    )
```

profile of v0, /device:TPU:1, one launch (start us, length us, event | category | flops | bytes accessed | tf_op | source)
XLA Modules:
  0.0 61.6 jit_solution(4380507642883123412)
XLA Ops:
  0.6 58.3 %shard_map.158 = (bf16[128,256]{1,0:T(8,128)(2,1)S(1)}, f32[16,2,128,256]{3,2,1,0:T(8,128)S(1)}) custom-call(bf16[128,256]{1,0:T(8,128)(2,1)} %tokens_ref.1, bf16[256]{0:T(256)(128)(2,1)} %norm_gain_ref.1, bf16[256,256]{1,0:T(8,128)(2,1)} %wq_hbm.1, bf16[256,256]{1,0:T(8,128)(2,1)} %wk_hbm.1, bf16[256,512]{1,0:T(8,128)(2,1)} %wv_hbm.1, ...), custom_call_target="tpu_custom_call" | custom-call | tf_op jit(solution)/shard_map/pallas_call | solution.py:475
  59.0 0.6 %copy.19 = bf16[128,256]{1,0:T(8,128)(2,1)} copy(bf16[128,256]{1,0:T(8,128)(2,1)S(1)} %get-tuple-element.2) | data formatting | bytes 131072
  59.6 2.0 %copy.20 = f32[16,2,128,256]{3,2,1,0:T(8,128)} copy(f32[16,2,128,256]{3,2,1,0:T(8,128)S(1)} %get-tuple-element.3) | data formatting | bytes 8388608
where the time goes:
time: 61.8 us; the launch traced here: 61.6 us
  Pallas kernels  58.3 us (94%)
  local copies, waits for them, and re-layouts  2.64 us (4%)
  between operations  0.64 us (1%)
    pallas_call x1, Pallas kernels, body(): pl.pallas_call(functools.partial(kernel, n_kv, n_tp, feats * n_kv), out_s...  58.3 us
    unnamed x2, local copies, waits for them, and re-layouts  2.64 us

commit v1 on v0

v1 whole, which is shorter than its diff:
```python
import functools

import jax
import jax.numpy as jnp
from jax import lax
from jax.experimental import pallas as pl
from jax.experimental.pallas import tpu as pltpu
from jax.sharding import PartitionSpec as P

eps = 1e-06
gate_norm = 16.0
LANES = 128
SUBLANES = 8
FF_SIZES = (1, 1, 2, 2, 2, 2, 1)
LAG_Z = 0
LAG_X = 2
AX, AZ, BZ, BX, CY, DX, DZ, EZ, EX, FY, SQX, SQZ, PHASES = 0, 1, 2, 3, 4, 5, 6, 7, 8, 9, 10, 12, 14
F32 = jnp.float32
BF16 = jnp.bfloat16


def remote(src, dst, send_sem, recv_sem, device):
    return pltpu.make_async_remote_copy(
        src_ref=src,
        dst_ref=dst,
        send_sem=send_sem,
        recv_sem=recv_sem,
        device_id=device,
        device_id_type=pl.DeviceIdType.MESH,
    )


def split_axis(n_kv):
    n_in = 1
    while n_in * n_in * 4 <= n_kv:
        n_in *= 2
    return n_kv // n_in, n_in


def ff_chunks(width):
    if width % LANES:
        return [(0, width)]
    left, sizes, k = width // LANES, [], 0
    while left:
        take = min(left, FF_SIZES[min(k, len(FF_SIZES) - 1)])
        sizes.append(take)
        left -= take
        k += 1
    at, ranges = 0, []
    for take in sizes:
        ranges.append((at, at + take * LANES))
        at += take * LANES
    return ranges


def proj_layout(kw, vw, dk, dv):
    heads = kw // dk
    at, chunks, where = 0, [], []

    def put(items):
        nonlocal at
        pieces, places = [], []
        for weight, lo, width in items:
            pieces.append((weight, lo, width, at))
            places.append(at)
            at += width
        chunks.append(pieces)
        return places

    for h in range(heads):
        q, k = put([("q", h * dk, dk), ("k", h * dk, dk)])
        d, v = put([("d", h * dk, dk), ("v", h * dv, dv)])
        where.append((q, k, d, v))
    (g,) = put([("g", 0, vw)])
    return chunks, where, g, at


def kernel(
    n_kv,
    n_tp,
    d_model,
    tokens_hbm,
    norm_gain_hbm,
    wq_hbm,
    wk_hbm,
    wv_hbm,
    wg_hbm,
    wd_hbm,
    log_decay_hbm,
    state_hbm,
    out_gain_hbm,
    wo_hbm,
    mixer_gain_hbm,
    wfg_hbm,
    wfu_hbm,
    wdn_hbm,
    result_ref,
    ns_ref,
    tokens_ref,
    norm_gain_ref,
    log_decay_ref,
    out_gain_ref,
    mixer_gain_ref,
    wall,
    wo,
    wff,
    wdn,
    sqx,
    sqz,
    px,
    rx,
    pz,
    rz,
    att,
    mg,
    to,
    fx,
    frx,
    fz,
    frz,
    hg,
    td,
    middle_ref,
    in_sem,
    w_sem,
    bulk_sem,
    send_sem,
    sq_r,
    ax_r,
    az_r,
    mz_r,
    t_r,
    fx_r,
    fz_r,
    hz_r,
    hx_r,
):
    n_out, n_in = split_axis(n_kv)
    kv = lax.axis_index("kv")
    tp = lax.axis_index("tp")
    zi = kv // n_in
    xi = lax.rem(kv, n_in)
    rows = px.shape[2]
    batch, feats = tokens_ref.shape
    heads, dk, dv = ns_ref.shape[1:]
    kw = wq_hbm.shape[1]
    vw = wv_hbm.shape[1]
    ff = wfg_hbm.shape[1]

    def x_peer(d):
        return lax.rem(xi + d, n_in)

    def z_peer(d):
        return lax.rem(zi + d, n_out)

    def z_back(d):
        return lax.rem(zi + n_out - d, n_out)

    def x_dev(d):
        return (zi * n_in + x_peer(d), tp)

    def z_dev(d):
        return (z_peer(d) * n_in + xi, tp)

    def t_dev(d):
        return (kv, lax.rem(tp + d, n_tp))

    barrier = pltpu.get_barrier_semaphore()
    peers = (
        [z_dev(d) for d in range(1, n_out)]
        + [x_dev(d) for d in range(1, n_in)]
        + [t_dev(d) for d in range(1, n_tp)]
    )
    for dev in peers:
        pl.semaphore_signal(barrier, inc=1, device_id=dev, device_id_type=pl.DeviceIdType.MESH)

    def fetch(src, dst, sem):
        copy = pltpu.make_async_copy(src, dst, sem)
        copy.start()
        return copy

    chunks, where, g_at, width = proj_layout(kw, vw, dk, dv)
    source = {"q": wq_hbm, "k": wk_hbm, "d": wd_hbm, "v": wv_hbm, "g": wg_hbm}
    first_loads = [
        fetch(tokens_hbm, tokens_ref, in_sem.at[0]),
        fetch(norm_gain_hbm, norm_gain_ref, in_sem.at[1]),
    ]
    bounds = []
    for c, pieces in enumerate(chunks):
        for name, lo, wide, at in pieces:
            fetch(source[name].at[:, lo : lo + wide], wall.at[:, at : at + wide], w_sem.at[c])
        bounds.append((pieces[0][3], pieces[-1][3] + pieces[-1][2]))

    def took(ref, sem):
        pltpu.make_async_copy(ref, ref, sem).wait()

    def launch(phase, src, dst, recv_sem, device):
        remote(src, dst, send_sem.at[phase], recv_sem, device).start()

    def scatter_rows(dst, value, lo):
        wide = value.shape[1]
        value = value.astype(BF16)
        for z in range(n_out):
            for x in range(n_in):
                at = (z * n_in + x) * rows
                dst[x, z, :, lo : lo + wide] = value[at : at + rows]

    def send_x(phase, src, dst, sem, lo, hi):
        for d in range(1, n_in):
            launch(
                phase,
                src.at[x_peer(d), :, :, lo:hi],
                dst.at[d - 1, :, :, lo:hi],
                sem,
                x_dev(d),
            )

    def send_z(phase, src, dst, sem, lo, hi):
        for d in range(1, n_out):
            launch(
                phase,
                src.at[z_peer(d), :, lo:hi],
                dst.at[d - 1, :, lo:hi],
                sem,
                z_dev(d),
            )

    def reduce_x(src, got, dst, sem, lo, hi):
        total = src[xi, :, :, lo:hi].astype(F32)
        if n_in > 1:
            took(got.at[:, :, :, lo:hi], sem)
            for d in range(1, n_in):
                total = total + got[d - 1, :, :, lo:hi].astype(F32)
        dst[:, :, lo:hi] = total.astype(BF16)

    def reduce_z(src, got, sem, lo, hi):
        total = src[zi, :, lo:hi].astype(F32)
        if n_out > 1:
            took(got.at[:, :, lo:hi], sem)
            for d in range(1, n_out):
                total = total + got[d - 1, :, lo:hi].astype(F32)
        return total

    def squares_x(i, values):
        ones = jnp.ones((SUBLANES, feats), F32)
        sqx[i, 0] = lax.dot_general(
            ones,
            values * values,
            (((1,), (1,)), ((), ())),
            precision=lax.Precision.HIGHEST,
            preferred_element_type=F32,
        )
        for d in range(1, n_in):
            launch(SQX + i, sqx.at[i, 0], sqx.at[i, d], sq_r.at[i, 0], x_dev(d))

    def squares_z(i):
        if n_in > 1:
            took(sqx.at[i, 1:n_in], sq_r.at[i, 0])
        total = sqx[i, 0]
        for d in range(1, n_in):
            total = total + sqx[i, d]
        sqz[i, 0] = total
        for d in range(1, n_out):
            launch(SQZ + i, sqz.at[i, 0], sqz.at[i, d], sq_r.at[i, 1], z_dev(d))

    def inverse(i):
        if n_out > 1:
            took(sqz.at[i, 1:n_out], sq_r.at[i, 1])
        total = sqz[i, 0]
        for d in range(1, n_out):
            total = total + sqz[i, d]
        lane = lax.broadcasted_iota(jnp.int32, (rows, batch), 1)
        mine = lax.broadcasted_iota(jnp.int32, (rows, batch), 0) + kv * rows
        own = jnp.where(lane == mine, jnp.broadcast_to(total[:1], (rows, batch)), 0.0)
        return lax.rsqrt(jnp.sum(own, axis=1, keepdims=True) / d_model + eps)

    for load in first_loads:
        load.wait()
    wide = tokens_ref[...].astype(F32)
    scaled = (wide * norm_gain_ref[...].astype(F32).reshape(1, -1)).astype(BF16)

    for c, (lo, hi) in enumerate(bounds):
        took(wall.at[:, lo:hi], w_sem.at[c])
        scatter_rows(px, jnp.dot(scaled, wall[:, lo:hi], preferred_element_type=F32), lo)
        if c == 0:
            pl.semaphore_wait(barrier, len(peers))
        send_x(AX, px, rx, ax_r.at[c], lo, hi)
        if c == 0:
            squares_x(0, wide)
    load_decay = fetch(log_decay_hbm, log_decay_ref, in_sem.at[0])
    load_gain = fetch(out_gain_hbm, out_gain_ref, in_sem.at[1])
    load_mixer = fetch(mixer_gain_hbm, mixer_gain_ref, in_sem.at[2])
    load_state = fetch(state_hbm, ns_ref, bulk_sem.at[0])
    load_o = fetch(wo_hbm, wo, bulk_sem.at[1])
    fchunks = ff_chunks(ff)
    n_c = len(fchunks)
    fbounds = [(2 * lo, 2 * hi) for lo, hi in fchunks]
    for lo, hi in fchunks:
        fetch(wfg_hbm.at[:, lo:hi], wff.at[:, 2 * lo : lo + hi], bulk_sem.at[2])
        fetch(wfu_hbm.at[:, lo:hi], wff.at[:, lo + hi : 2 * hi], bulk_sem.at[2])
    load_dn = fetch(wdn_hbm, wdn, bulk_sem.at[3])

    for c, (lo, hi) in enumerate(bounds):
        reduce_x(px, rx, pz, ax_r.at[c], lo, hi)
        send_z(AZ, pz, rz, az_r.at[c], lo, hi)
        if c == 0:
            squares_z(0)

    load_decay.wait()
    load_state.wait()
    inv = None
    for h in range(heads):
        c = 2 * h
        q_at, k_at, d_at, v_at = (at for at in where[h])
        qk = reduce_z(pz, rz, az_r.at[c], *bounds[c])
        if h == 0:
            inv = inverse(0)
        qk = qk * inv
        dv_terms = reduce_z(pz, rz, az_r.at[c + 1], *bounds[c + 1]) * inv
        query = qk[:, :dk] * dk ** (-0.5)
        pre = dv_terms[:, :dk]
        values = dv_terms[:, dk:]
        log_sig = jnp.minimum(pre, 0.0) - jnp.log1p(jnp.exp(-jnp.abs(pre)))
        decay = jnp.exp(log_sig / gate_norm + log_decay_ref[:, h * dk : (h + 1) * dk])
        q_t = query.T
        k_t = qk[:, dk:].T
        a_t = decay.T
        for b in range(rows):
            col = slice(b, b + 1)
            new = ns_ref[b, h] * a_t[:, col] + k_t[:, col] * values[col, :]
            ns_ref[b, h] = new
            att[h, col, :] = jnp.sum(new * q_t[:, col], axis=0, keepdims=True)

    load_gain.wait()
    last = len(bounds) - 1
    gate = reduce_z(pz, rz, az_r.at[last], *bounds[last]) * inv
    for h in range(heads):
        got = att[h]
        normed = (
            got
            * lax.rsqrt(jnp.mean(got * got, axis=1, keepdims=True) + eps)
            * out_gain_ref[...]
        )
        cols = slice(h * dv, (h + 1) * dv)
        mg[zi, xi, :, cols] = (normed * jax.nn.silu(gate[:, cols])).astype(BF16)

    own = mg.at[zi, xi]
    for d in range(1, n_out):
        launch(BZ, own, own, mz_r.at[d - 1], z_dev(d))
    for dz in range(n_out):
        slot = mg.at[z_back(dz), xi]
        if dz:
            took(slot, mz_r.at[dz - 1])
        for d in range(1, n_in):
            launch(BX, slot, slot, t_r.at[2], x_dev(d))
    load_o.wait()
    if n_in > 1:
        took(mg.at[:, : n_in - 1], t_r.at[2])

    def sum_groups(phase, buf, sem):
        for d in range(1, n_tp):
            launch(phase, buf.at[tp], buf.at[tp], sem, t_dev(d))
        if n_tp > 1:
            took(buf.at[: n_tp - 1], sem)
        total = buf[0].astype(F32)
        for g in range(1, n_tp):
            total = total + buf[g].astype(F32)
        return total

    mixed = mg[...].reshape(batch, vw)
    to[tp] = jnp.dot(mixed, wo[...], preferred_element_type=F32).astype(BF16)
    middle = (tokens_ref[...].astype(F32) + sum_groups(CY, to, t_r.at[0])).astype(BF16)
    middle_ref[...] = middle

    load_mixer.wait()
    wide2 = middle.astype(F32)
    scaled2 = (wide2 * mixer_gain_ref[...].astype(F32).reshape(1, -1)).astype(BF16)
    took(wff, bulk_sem.at[2])
    for c, (lo, hi) in enumerate(fbounds):
        scatter_rows(fx, jnp.dot(scaled2, wff[:, lo:hi], preferred_element_type=F32), lo)
        send_x(DX, fx, frx, fx_r.at[c], lo, hi)
        if c == 0:
            squares_x(1, wide2)

    inv2 = [None]

    def to_z(c):
        lo, hi = fbounds[c]
        reduce_x(fx, frx, fz, fx_r.at[c], lo, hi)
        send_z(DZ, fz, frz, fz_r.at[c], lo, hi)
        if c == 0:
            squares_z(1)

    def activate(c):
        terms = reduce_z(fz, frz, fz_r.at[c], *fbounds[c])
        if c == 0:
            inv2[0] = inverse(1)
        terms = terms * inv2[0]
        fc = terms.shape[1] // 2
        cols = slice(*fchunks[c])
        hg[zi, xi, :, cols] = (jax.nn.silu(terms[:, :fc]) * terms[:, fc:]).astype(BF16)
        own = hg.at[zi, xi, :, cols]
        for d in range(1, n_out):
            launch(EZ, own, own, hz_r.at[c], z_dev(d))

    def hand_on(c):
        cols = slice(*fchunks[c])
        if n_out > 1:
            took(hg.at[: n_out - 1, 0, :, cols], hz_r.at[c])
        slot = hg.at[:, xi, :, cols]
        for d in range(1, n_in):
            launch(EX, slot, slot, hx_r.at[c], x_dev(d))

    lag_z = n_c + LAG_Z
    lag_x = lag_z + LAG_X
    for t in range(n_c + lag_x):
        if t < n_c:
            to_z(t)
        if 0 <= t - lag_z < n_c:
            activate(t - lag_z)
        if 0 <= t - lag_x < n_c:
            hand_on(t - lag_x)

    load_dn.wait()
    down = None
    for c, (lo, hi) in enumerate(fchunks):
        if n_in > 1:
            took(hg.at[:, : n_in - 1, :, lo:hi], hx_r.at[c])
        term = jnp.dot(
            hg[:, :, :, lo:hi].reshape(batch, hi - lo),
            wdn[lo:hi, :],
            preferred_element_type=F32,
        )
        down = term if down is None else down + term
    td[tp] = down.astype(BF16)
    total = sum_groups(FY, td, t_r.at[1])
    result_ref[...] = (middle_ref[...].astype(F32) + total).astype(BF16)

    if n_in > 1:
        took(rx, send_sem.at[AX])
        took(frx, send_sem.at[DX])
        took(mg.at[:, : n_in - 1], send_sem.at[BX])
        took(hg.at[:, : n_in - 1], send_sem.at[EX])
        for i in range(2):
            took(sqx.at[i, 1:n_in], send_sem.at[SQX + i])
    if n_out > 1:
        took(rz, send_sem.at[AZ])
        took(frz, send_sem.at[DZ])
        took(mg.at[: n_out - 1, 0], send_sem.at[BZ])
        took(hg.at[: n_out - 1, 0], send_sem.at[EZ])
        for i in range(2):
            took(sqz.at[i, 1:n_out], send_sem.at[SQZ + i])
    if n_tp > 1:
        took(to.at[: n_tp - 1], send_sem.at[CY])
        took(td.at[: n_tp - 1], send_sem.at[FY])


def body(n_kv, n_tp, *args):
    (
        tokens,
        norm_gain,
        w_query,
        w_key,
        w_value,
        w_gate,
        w_decay,
        log_decay,
        state,
        out_gain,
        w_out,
        mixer_gain,
        w_ffgate,
        w_ffup,
        w_down,
    ) = args
    n_out, n_in = split_axis(n_kv)
    batch, feats = tokens.shape
    rows, heads, dk, dv = state.shape
    kw = w_query.shape[1]
    vw = w_value.shape[1]
    ff = w_ffgate.shape[1]
    n_c = len(ff_chunks(ff))
    chunks, _, _, width = proj_layout(kw, vw, dk, dv)
    n_a = len(chunks)
    m_in, m_out = max(n_in - 1, 1), max(n_out - 1, 1)
    dma = pltpu.SemaphoreType.DMA
    vmem = pltpu.VMEM
    whole = pl.BlockSpec(memory_space=pltpu.VMEM)
    far = pl.BlockSpec(memory_space=pl.ANY)
    sems = [
        (3,),
        (n_a,),
        (4,),
        (PHASES,),
        (2, 2),
        (n_a,),
        (n_a,),
        (m_out,),
        (3,),
        (n_c,),
        (n_c,),
        (n_c,),
        (n_c,),
    ]
    result, new_state = pl.pallas_call(
        functools.partial(kernel, n_kv, n_tp, feats * n_kv),
        out_shape=(
            vmem((batch, feats), BF16),
            vmem(state.shape, F32),
        ),
        in_specs=[far] * 15,
        out_specs=(whole, whole),
        scratch_shapes=[
            vmem((batch, feats), BF16),
            vmem(norm_gain.shape, BF16),
            vmem(log_decay.shape, F32),
            vmem((1, dv), F32),
            vmem(mixer_gain.shape, BF16),
            vmem((feats, width), BF16),
            vmem(w_out.shape, BF16),
            vmem((feats, 2 * ff), BF16),
            vmem(w_down.shape, BF16),
            vmem((2, n_in, SUBLANES, batch), F32),
            vmem((2, n_out, SUBLANES, batch), F32),
            vmem((n_in, n_out, rows, width), BF16),
            vmem((m_in, n_out, rows, width), BF16),
            vmem((n_out, rows, width), BF16),
            vmem((m_out, rows, width), BF16),
            vmem((heads, rows, dv), F32),
            vmem((n_out, n_in, rows, vw), BF16),
            vmem((n_tp, batch, feats), BF16),
            vmem((n_in, n_out, rows, 2 * ff), BF16),
            vmem((m_in, n_out, rows, 2 * ff), BF16),
            vmem((n_out, rows, 2 * ff), BF16),
            vmem((m_out, rows, 2 * ff), BF16),
            vmem((n_out, n_in, rows, ff), BF16),
            vmem((n_tp, batch, feats), BF16),
            vmem((batch, feats), BF16),
        ]
        + [dma(shape) for shape in sems],
        compiler_params=pltpu.CompilerParams(
            collective_id=0, has_side_effects=True, vmem_limit_bytes=56 * 2**20
        ),
    )(
        tokens,
        norm_gain,
        w_query,
        w_key,
        w_value,
        w_gate,
        w_decay,
        log_decay,
        state,
        out_gain.reshape(1, dv),
        w_out,
        mixer_gain,
        w_ffgate,
        w_ffup,
        w_down,
    )
    return (result, new_state)


def solution(mesh):
    return jax.shard_map(
        functools.partial(body, mesh.shape["kv"], mesh.shape["tp"]),
        mesh=mesh,
        in_specs=(
            P(None, "kv"),
            P("kv"),
            P("kv", "tp"),
            P("kv", "tp"),
            P("kv", "tp"),
            P("kv", "tp"),
            P("kv", "tp"),
            P("kv", "tp"),
            P("kv", "tp", None, None),
            P(),
            P("tp", "kv"),
            P("kv"),
            P("kv", "tp"),
            P("kv", "tp"),
            P("tp", "kv"),
        ),
        out_specs=(P(None, "kv"), P("kv", "tp", None, None)),
        check_vma=False,
    )
```

time: 61.8 us -> 60 us (0.971)
  Pallas kernels: 58.3 us -> 56.6 us
    pallas_call x1, Pallas kernels: 58.3 us -> 56.6 us  [body(): pl.pallas_call(functools.partial(kernel, n_kv, n_tp, feats * n_kv), out_s...]
where the time goes in v1:
time: 60 us; the launch traced here: 59.8 us
  Pallas kernels  56.6 us (94%)
  local copies, waits for them, and re-layouts  2.64 us (4%)
  between operations  0.64 us (1%)
    pallas_call x1, Pallas kernels, body(): pl.pallas_call(functools.partial(kernel, n_kv, n_tp, feats * n_kv), out_s...  56.6 us
    unnamed x2, local copies, waits for them, and re-layouts  2.64 us

profile of v1, /device:TPU:1, one launch (start us, length us, event | category | flops | bytes accessed | tf_op | source)
XLA Modules:
  0.0 59.8 jit_solution(13591278598658916340)
XLA Ops:
  0.6 56.6 %shard_map.158 = (bf16[128,256]{1,0:T(8,128)(2,1)S(1)}, f32[16,2,128,256]{3,2,1,0:T(8,128)S(1)}) custom-call(bf16[128,256]{1,0:T(8,128)(2,1)} %tokens_hbm.1, bf16[256]{0:T(256)(128)(2,1)} %norm_gain_hbm.1, bf16[256,256]{1,0:T(8,128)(2,1)} %wq_hbm.1, bf16[256,256]{1,0:T(8,128)(2,1)} %wk_hbm.1, bf16[256,512]{1,0:T(8,128)(2,1)} %wv_hbm.1, ...), custom_call_target="tpu_custom_call" | custom-call | tf_op jit(solution)/shard_map/pallas_call | solution.py:505
  57.2 0.6 %copy.19 = bf16[128,256]{1,0:T(8,128)(2,1)} copy(bf16[128,256]{1,0:T(8,128)(2,1)S(1)} %get-tuple-element.2) | data formatting | bytes 131072
  57.8 2.0 %copy.20 = f32[16,2,128,256]{3,2,1,0:T(8,128)} copy(f32[16,2,128,256]{3,2,1,0:T(8,128)S(1)} %get-tuple-element.3) | data formatting | bytes 8388608

commit v2 on v1

--- a/solution.py
+++ b/solution.py
@@ -11,10 +11,17 @@
 gate_norm = 16.0
 LANES = 128
 SUBLANES = 8
-FF_SIZES = (1, 1, 2, 2, 2, 2, 1)
-LAG_Z = 0
-LAG_X = 2
-AX, AZ, BZ, BX, CY, DX, DZ, EZ, EX, FY, SQX, SQZ, PHASES = 0, 1, 2, 3, 4, 5, 6, 7, 8, 9, 10, 12, 14
+FF_SIZES = (1, 1, 2, 2, 2, 1)
+FF_Z = 2
+LAG_ZX = 7
+SQ_AT = 1
+A_ZF = 1
+LAG_ZACT = 11
+LAG_ACT = 9
+LAG_RELAY = 50
+LAG_HAND = 100
+DIRECT = 99
+AX, AZ, BZ, BX, CY, DX, DZ, EZ, EX, FY, SQX, SQZ, ZF, XF, PHASES = 0, 1, 2, 3, 4, 5, 6, 7, 8, 9, 10, 12, 14, 16, 18
 F32 = jnp.float32
 BF16 = jnp.bfloat16
 
@@ -37,15 +44,19 @@
     return n_kv // n_in, n_in
 
 
-def ff_chunks(width):
+def ff_chunks(width, z_units):
     if width % LANES:
         return [(0, width)]
-    left, sizes, k = width // LANES, [], 0
+    units = width // LANES
+    tail = z_units if z_units < units else 0
+    left, sizes, k = units - tail, [], 0
     while left:
         take = min(left, FF_SIZES[min(k, len(FF_SIZES) - 1)])
         sizes.append(take)
         left -= take
         k += 1
+    if tail:
+        sizes.append(tail)
     at, ranges = 0, []
     for take in sizes:
         ranges.append((at, at + take * LANES))
@@ -114,6 +125,7 @@
     att,
     mg,
     to,
+    away,
     fx,
     frx,
     fz,
@@ -121,6 +133,12 @@
     hg,
     td,
     middle_ref,
+    zfr,
+    zfs,
+    zfx,
+    dfr,
+    dfs,
+    dfx,
     in_sem,
     w_sem,
     bulk_sem,
@@ -133,7 +151,9 @@
     fx_r,
     fz_r,
     hz_r,
+    hp_r,
     hx_r,
+    zf_r,
 ):
     n_out, n_in = split_axis(n_kv)
     kv = lax.axis_index("kv")
@@ -165,12 +185,13 @@
     def t_dev(d):
         return (kv, lax.rem(tp + d, n_tp))
 
+    def xt_dev(d, e):
+        return (zi * n_in + x_peer(d), lax.rem(tp + e, n_tp))
+
     barrier = pltpu.get_barrier_semaphore()
-    peers = (
-        [z_dev(d) for d in range(1, n_out)]
-        + [x_dev(d) for d in range(1, n_in)]
-        + [t_dev(d) for d in range(1, n_tp)]
-    )
+    peers = [z_dev(d) for d in range(1, n_out)] + [
+        xt_dev(d, e) for d in range(n_in) for e in range(n_tp) if d or e
+    ]
     for dev in peers:
         pl.semaphore_signal(barrier, inc=1, device_id=dev, device_id_type=pl.DeviceIdType.MESH)
 
@@ -186,9 +207,13 @@
         fetch(norm_gain_hbm, norm_gain_ref, in_sem.at[1]),
     ]
     bounds = []
-    for c, pieces in enumerate(chunks):
-        for name, lo, wide, at in pieces:
+    two_way = n_in > 1 and n_out > 1
+    a_zf = 2 * (heads - 1) if two_way and A_ZF else None
+    order = [0] + sorted(range(1, len(chunks)), key=lambda c: (c != a_zf, c))
+    for c in order:
+        for name, lo, wide, at in chunks[c]:
             fetch(source[name].at[:, lo : lo + wide], wall.at[:, at : at + wide], w_sem.at[c])
+    for pieces in chunks:
         bounds.append((pieces[0][3], pieces[-1][3] + pieces[-1][2]))
 
     def took(ref, sem):
@@ -239,6 +264,26 @@
             took(got.at[:, :, lo:hi], sem)
             for d in range(1, n_out):
                 total = total + got[d - 1, :, lo:hi].astype(F32)
+        return total
+
+    def zf_send(i, src, dst, lo, hi):
+        for d in range(1, n_out):
+            launch(ZF + i, src.at[:, z_peer(d), :, lo:hi], dst.at[d - 1], zf_r.at[i, 0], z_dev(d))
+
+    def zf_to_x(i, src, got, mid, dst, lo, hi):
+        took(got, zf_r.at[i, 0])
+        total = src[:, zi, :, lo:hi].astype(F32)
+        for d in range(1, n_out):
+            total = total + got[d - 1].astype(F32)
+        mid[...] = total.astype(BF16)
+        for d in range(1, n_in):
+            launch(XF + i, mid.at[x_peer(d)], dst.at[d - 1], zf_r.at[i, 1], x_dev(d))
+
+    def zf_final(i, mid, got):
+        took(got, zf_r.at[i, 1])
+        total = mid[xi].astype(F32)
+        for d in range(1, n_in):
+            total = total + got[d - 1].astype(F32)
         return total
 
     def squares_x(i, values):
@@ -279,32 +324,50 @@
     wide = tokens_ref[...].astype(F32)
     scaled = (wide * norm_gain_ref[...].astype(F32).reshape(1, -1)).astype(BF16)
 
-    for c, (lo, hi) in enumerate(bounds):
+    for k, c in enumerate(order):
+        lo, hi = bounds[c]
         took(wall.at[:, lo:hi], w_sem.at[c])
         scatter_rows(px, jnp.dot(scaled, wall[:, lo:hi], preferred_element_type=F32), lo)
-        if c == 0:
+        if k == 0:
             pl.semaphore_wait(barrier, len(peers))
-        send_x(AX, px, rx, ax_r.at[c], lo, hi)
-        if c == 0:
+        if c == a_zf:
+            zf_send(0, px, zfr, lo, hi)
+        else:
+            send_x(AX, px, rx, ax_r.at[c], lo, hi)
+        if k == 1:
             squares_x(0, wide)
     load_decay = fetch(log_decay_hbm, log_decay_ref, in_sem.at[0])
     load_gain = fetch(out_gain_hbm, out_gain_ref, in_sem.at[1])
     load_mixer = fetch(mixer_gain_hbm, mixer_gain_ref, in_sem.at[2])
     load_state = fetch(state_hbm, ns_ref, bulk_sem.at[0])
-    load_o = fetch(wo_hbm, wo, bulk_sem.at[1])
-    fchunks = ff_chunks(ff)
+    load_o = fetch(wo_hbm, wo.at[xi], bulk_sem.at[1])
+    fchunks = ff_chunks(ff, FF_Z if two_way else 0)
     n_c = len(fchunks)
+    d_zf = n_c - 1 if two_way and n_c > 1 else None
     fbounds = [(2 * lo, 2 * hi) for lo, hi in fchunks]
     for lo, hi in fchunks:
         fetch(wfg_hbm.at[:, lo:hi], wff.at[:, 2 * lo : lo + hi], bulk_sem.at[2])
         fetch(wfu_hbm.at[:, lo:hi], wff.at[:, lo + hi : 2 * hi], bulk_sem.at[2])
     load_dn = fetch(wdn_hbm, wdn, bulk_sem.at[3])
 
-    for c, (lo, hi) in enumerate(bounds):
+    x_order = [c for c in order if c != a_zf]
+    for k, c in enumerate(x_order):
+        lo, hi = bounds[c]
+        if a_zf is not None and k == len(x_order) - 1:
+            zf_to_x(0, px, zfr, zfs, zfx, *bounds[a_zf])
         reduce_x(px, rx, pz, ax_r.at[c], lo, hi)
         send_z(AZ, pz, rz, az_r.at[c], lo, hi)
-        if c == 0:
+        if k == 1:
             squares_z(0)
+
+    for d in range(1, n_in):
+        launch(BX, wo_hbm, wo.at[xi], t_r.at[2], x_dev(d))
+
+    def arrived(c):
+        if c == a_zf:
+            return zf_final(0, zfs, zfx)
+        return reduce_z(pz, rz, az_r.at[c], *bounds[c])
+
 
     load_decay.wait()
     load_state.wait()
@@ -312,11 +375,11 @@
     for h in range(heads):
         c = 2 * h
         q_at, k_at, d_at, v_at = (at for at in where[h])
-        qk = reduce_z(pz, rz, az_r.at[c], *bounds[c])
+        qk = arrived(c)
         if h == 0:
             inv = inverse(0)
         qk = qk * inv
-        dv_terms = reduce_z(pz, rz, az_r.at[c + 1], *bounds[c + 1]) * inv
+        dv_terms = arrived(c + 1) * inv
         query = qk[:, :dk] * dk ** (-0.5)
         pre = dv_terms[:, :dk]
         values = dv_terms[:, dk:]
@@ -342,20 +405,44 @@
             * out_gain_ref[...]
         )
         cols = slice(h * dv, (h + 1) * dv)
-        mg[zi, xi, :, cols] = (normed * jax.nn.silu(gate[:, cols])).astype(BF16)
-
-    own = mg.at[zi, xi]
+        mg[zi, :, cols] = (normed * jax.nn.silu(gate[:, cols])).astype(BF16)
+
+    own = mg.at[zi]
     for d in range(1, n_out):
-        launch(BZ, own, own, mz_r.at[d - 1], z_dev(d))
-    for dz in range(n_out):
-        slot = mg.at[z_back(dz), xi]
-        if dz:
-            took(slot, mz_r.at[dz - 1])
-        for d in range(1, n_in):
-            launch(BX, slot, slot, t_r.at[2], x_dev(d))
+        launch(BZ, own, own, mz_r.at[0], z_dev(d))
     load_o.wait()
     if n_in > 1:
-        took(mg.at[:, : n_in - 1], t_r.at[2])
+        took(wo.at[: n_in - 1], t_r.at[2])
+    if n_out > 1:
+        took(mg.at[: n_out - 1], mz_r.at[0])
+    mixed = mg[...].reshape(n_out * rows, vw)
+    mine = xi * n_tp + tp
+    for d in range(1, n_in):
+        part = jnp.dot(mixed, wo[x_peer(d)], preferred_element_type=F32)
+        away[d - 1] = part.astype(BF16)
+        for e in range(n_tp):
+            launch(CY, away.at[d - 1], to.at[mine], t_r.at[3], xt_dev(d, e))
+    to[mine] = jnp.dot(mixed, wo[xi], preferred_element_type=F32).astype(BF16)
+    for e in range(1, n_tp):
+        launch(CY, to.at[mine], to.at[mine], t_r.at[0], t_dev(e))
+
+    def heads_sum(x):
+        total = to[x * n_tp].astype(F32)
+        for g in range(1, n_tp):
+            total = total + to[x * n_tp + g].astype(F32)
+        tok = jnp.stack(
+            [tokens_ref[pl.ds((z * n_in + x) * rows, rows), :] for z in range(n_out)]
+        )
+        return (tok.astype(F32) + total.reshape(n_out, rows, feats)).astype(BF16)
+
+    if n_tp > 1:
+        took(to.at[: n_tp - 1], t_r.at[0])
+    middle_ref[:, xi] = heads_sum(xi)
+    if n_in > 1:
+        took(to.at[: (n_in - 1) * n_tp], t_r.at[3])
+    for d in range(1, n_in):
+        middle_ref[:, x_peer(d)] = heads_sum(x_peer(d))
+    middle = middle_ref[...].reshape(batch, feats)
 
     def sum_groups(phase, buf, sem):
         for d in range(1, n_tp):
@@ -367,59 +454,91 @@
             total = total + buf[g].astype(F32)
         return total
 
-    mixed = mg[...].reshape(batch, vw)
-    to[tp] = jnp.dot(mixed, wo[...], preferred_element_type=F32).astype(BF16)
-    middle = (tokens_ref[...].astype(F32) + sum_groups(CY, to, t_r.at[0])).astype(BF16)
-    middle_ref[...] = middle
-
     load_mixer.wait()
     wide2 = middle.astype(F32)
     scaled2 = (wide2 * mixer_gain_ref[...].astype(F32).reshape(1, -1)).astype(BF16)
     took(wff, bulk_sem.at[2])
-    for c, (lo, hi) in enumerate(fbounds):
+    d_order = list(range(n_c))
+    if d_zf is not None:
+        d_order = [0, d_zf] + list(range(1, d_zf))
+    for k, c in enumerate(d_order):
+        lo, hi = fbounds[c]
         scatter_rows(fx, jnp.dot(scaled2, wff[:, lo:hi], preferred_element_type=F32), lo)
-        send_x(DX, fx, frx, fx_r.at[c], lo, hi)
-        if c == 0:
+        if c == d_zf:
+            zf_send(1, fx, dfr, lo, hi)
+        else:
+            send_x(DX, fx, frx, fx_r.at[c], lo, hi)
+        if k == min(SQ_AT, n_c - 1):
             squares_x(1, wide2)
 
     inv2 = [None]
+    half = n_out // 2
+
+    def relayed(c):
+        return n_out % 2 == 0 and c < n_c - DIRECT
+
+    def near_dev(d):
+        base = (zi // half) * half
+        return ((base + lax.rem(zi - base + d, half)) * n_in + xi, tp)
 
     def to_z(c):
         lo, hi = fbounds[c]
         reduce_x(fx, frx, fz, fx_r.at[c], lo, hi)
         send_z(DZ, fz, frz, fz_r.at[c], lo, hi)
-        if c == 0:
+        if c == min(1, n_c - 2):
             squares_z(1)
 
     def activate(c):
-        terms = reduce_z(fz, frz, fz_r.at[c], *fbounds[c])
-        if c == 0:
+        if c == d_zf:
+            terms = zf_final(1, dfs, dfx)
+        else:
+            terms = reduce_z(fz, frz, fz_r.at[c], *fbounds[c])
+        if inv2[0] is None:
             inv2[0] = inverse(1)
         terms = terms * inv2[0]
         fc = terms.shape[1] // 2
         cols = slice(*fchunks[c])
         hg[zi, xi, :, cols] = (jax.nn.silu(terms[:, :fc]) * terms[:, fc:]).astype(BF16)
         own = hg.at[zi, xi, :, cols]
-        for d in range(1, n_out):
-            launch(EZ, own, own, hz_r.at[c], z_dev(d))
+        if not relayed(c):
+            for d in range(1, n_out):
+                launch(EZ, own, own, hz_r.at[c], z_dev(d))
+            return
+        for d in range(1, half):
+            launch(EZ, own, own, hz_r.at[c], near_dev(d))
+        launch(EZ, own, own, hp_r.at[c], z_dev(half))
+
+    def relay(c):
+        if not relayed(c):
+            return
+        cols = slice(*fchunks[c])
+        slot = hg.at[z_peer(half), xi, :, cols]
+        took(slot, hp_r.at[c])
+        for d in range(1, half):
+            launch(EZ, slot, slot, hz_r.at[c], near_dev(d))
 
     def hand_on(c):
         cols = slice(*fchunks[c])
-        if n_out > 1:
-            took(hg.at[: n_out - 1, 0, :, cols], hz_r.at[c])
+        far = 2 * (half - 1) if relayed(c) else n_out - 1
+        if far:
+            took(hg.at[:far, 0, :, cols], hz_r.at[c])
         slot = hg.at[:, xi, :, cols]
         for d in range(1, n_in):
             launch(EX, slot, slot, hx_r.at[c], x_dev(d))
 
-    lag_z = n_c + LAG_Z
-    lag_x = lag_z + LAG_X
-    for t in range(n_c + lag_x):
-        if t < n_c:
-            to_z(t)
-        if 0 <= t - lag_z < n_c:
-            activate(t - lag_z)
-        if 0 <= t - lag_x < n_c:
-            hand_on(t - lag_x)
+    steps = []
+    for c in range(n_c):
+        at = fchunks[c][1] / LANES
+        if c == d_zf:
+            steps.append((LAG_ZX, len(steps), lambda c: zf_to_x(1, fx, dfr, dfs, dfx, *fbounds[c]), c))
+            steps.append((LAG_ZACT, len(steps), activate, c))
+        else:
+            steps.append((at, len(steps), to_z, c))
+            steps.append((at + LAG_ACT, len(steps), activate, c))
+        steps.append((at + LAG_RELAY, len(steps), relay, c))
+        steps.append((at + LAG_HAND if c != d_zf else LAG_HAND, len(steps), hand_on, c))
+    for _, _, step, c in sorted(steps, key=lambda item: item[:2]):
+        step(c)
 
     load_dn.wait()
     down = None
@@ -434,24 +553,36 @@
         down = term if down is None else down + term
     td[tp] = down.astype(BF16)
     total = sum_groups(FY, td, t_r.at[1])
-    result_ref[...] = (middle_ref[...].astype(F32) + total).astype(BF16)
-
+    wide3 = middle_ref[...].reshape(batch, feats).astype(F32)
+    result_ref[...] = (wide3 + total).astype(BF16)
+
+    def sent_but(ref, phase, ranges, but):
+        left = sum(hi - lo for c, (lo, hi) in enumerate(ranges) if c != but)
+        took(ref.at[..., :left], send_sem.at[phase])
+
+    if a_zf is not None:
+        took(zfr, send_sem.at[ZF])
+        took(zfx, send_sem.at[XF])
+    if d_zf is not None:
+        took(dfr, send_sem.at[ZF + 1])
+        took(dfx, send_sem.at[XF + 1])
     if n_in > 1:
-        took(rx, send_sem.at[AX])
-        took(frx, send_sem.at[DX])
-        took(mg.at[:, : n_in - 1], send_sem.at[BX])
+        sent_but(rx, AX, bounds, a_zf)
+        sent_but(frx, DX, fbounds, d_zf)
+        took(wo.at[: n_in - 1], send_sem.at[BX])
         took(hg.at[:, : n_in - 1], send_sem.at[EX])
         for i in range(2):
             took(sqx.at[i, 1:n_in], send_sem.at[SQX + i])
     if n_out > 1:
-        took(rz, send_sem.at[AZ])
-        took(frz, send_sem.at[DZ])
-        took(mg.at[: n_out - 1, 0], send_sem.at[BZ])
+        sent_but(rz, AZ, bounds, a_zf)
+        sent_but(frz, DZ, fbounds, d_zf)
+        took(mg.at[: n_out - 1], send_sem.at[BZ])
         took(hg.at[: n_out - 1, 0], send_sem.at[EZ])
         for i in range(2):
             took(sqz.at[i, 1:n_out], send_sem.at[SQZ + i])
+    if n_in * n_tp > 1:
+        took(to.at[: n_in * n_tp - 1], send_sem.at[CY])
     if n_tp > 1:
-        took(to.at[: n_tp - 1], send_sem.at[CY])
         took(td.at[: n_tp - 1], send_sem.at[FY])
 
 
@@ -479,7 +610,11 @@
     kw = w_query.shape[1]
     vw = w_value.shape[1]
     ff = w_ffgate.shape[1]
-    n_c = len(ff_chunks(ff))
+    n_in_out = n_in > 1 and n_out > 1
+    fchunks = ff_chunks(ff, FF_Z if n_in_out else 0)
+    n_c = len(fchunks)
+    d_w = 2 * (fchunks[-1][1] - fchunks[-1][0])
+    a_w = 2 * dk
     chunks, _, _, width = proj_layout(kw, vw, dk, dv)
     n_a = len(chunks)
     m_in, m_out = max(n_in - 1, 1), max(n_out - 1, 1)
@@ -495,12 +630,14 @@
         (2, 2),
         (n_a,),
         (n_a,),
-        (m_out,),
-        (3,),
+        (1,),
+        (4,),
         (n_c,),
         (n_c,),
         (n_c,),
         (n_c,),
+        (n_c,),
+        (2, 2),
     ]
     result, new_state = pl.pallas_call(
         functools.partial(kernel, n_kv, n_tp, feats * n_kv),
@@ -517,7 +654,7 @@
             vmem((1, dv), F32),
             vmem(mixer_gain.shape, BF16),
             vmem((feats, width), BF16),
-            vmem(w_out.shape, BF16),
+            vmem((n_in,) + w_out.shape, BF16),
             vmem((feats, 2 * ff), BF16),
             vmem(w_down.shape, BF16),
             vmem((2, n_in, SUBLANES, batch), F32),
@@ -527,15 +664,22 @@
             vmem((n_out, rows, width), BF16),
             vmem((m_out, rows, width), BF16),
             vmem((heads, rows, dv), F32),
-            vmem((n_out, n_in, rows, vw), BF16),
-            vmem((n_tp, batch, feats), BF16),
+            vmem((n_out, rows, vw), BF16),
+            vmem((n_in * n_tp, n_out * rows, feats), BF16),
+            vmem((m_in, n_out * rows, feats), BF16),
             vmem((n_in, n_out, rows, 2 * ff), BF16),
             vmem((m_in, n_out, rows, 2 * ff), BF16),
             vmem((n_out, rows, 2 * ff), BF16),
             vmem((m_out, rows, 2 * ff), BF16),
             vmem((n_out, n_in, rows, ff), BF16),
             vmem((n_tp, batch, feats), BF16),
-            vmem((batch, feats), BF16),
+            vmem((n_out, n_in, rows, feats), BF16),
+            vmem((m_out, n_in, rows, a_w), BF16),
+            vmem((n_in, rows, a_w), BF16),
+            vmem((m_in, rows, a_w), BF16),
+            vmem((m_out, n_in, rows, d_w), BF16),
+            vmem((n_in, rows, d_w), BF16),
+            vmem((m_in, rows, d_w), BF16),
         ]
         + [dma(shape) for shape in sems],
         compiler_params=pltpu.CompilerParams(

time: 60 us -> 54 us (0.900)
  Pallas kernels: 56.6 us -> 50.6 us
    pallas_call x1, Pallas kernels: 56.6 us -> 50.6 us  [body(): pl.pallas_call(functools.partial(kernel, n_kv, n_tp, feats * n_kv), out_s...]
where the time goes in v2:
time: 54 us; the launch traced here: 53.9 us
  Pallas kernels  50.6 us (94%)
  local copies, waits for them, and re-layouts  2.64 us (5%)
  between operations  0.64 us (1%)
    pallas_call x1, Pallas kernels, body(): pl.pallas_call(functools.partial(kernel, n_kv, n_tp, feats * n_kv), out_s...  50.6 us
    unnamed x2, local copies, waits for them, and re-layouts  2.64 us

profile of v2, /device:TPU:1, one launch (start us, length us, event | category | flops | bytes accessed | tf_op | source)
XLA Modules:
  0.0 53.9 jit_solution(3597825506993602161)
XLA Ops:
  0.6 50.6 %shard_map.158 = (bf16[128,256]{1,0:T(8,128)(2,1)S(1)}, f32[16,2,128,256]{3,2,1,0:T(8,128)S(1)}) custom-call(bf16[128,256]{1,0:T(8,128)(2,1)} %tokens_hbm.1, bf16[256]{0:T(256)(128)(2,1)} %norm_gain_hbm.1, bf16[256,256]{1,0:T(8,128)(2,1)} %wq_hbm.1, bf16[256,256]{1,0:T(8,128)(2,1)} %wk_hbm.1, bf16[256,512]{1,0:T(8,128)(2,1)} %wv_hbm.1, ...), custom_call_target="tpu_custom_call" | custom-call | tf_op jit(solution)/shard_map/pallas_call | solution.py:642
  51.2 0.6 %copy.19 = bf16[128,256]{1,0:T(8,128)(2,1)} copy(bf16[128,256]{1,0:T(8,128)(2,1)S(1)} %get-tuple-element.2) | data formatting | bytes 131072
  51.9 2.0 %copy.20 = f32[16,2,128,256]{3,2,1,0:T(8,128)} copy(f32[16,2,128,256]{3,2,1,0:T(8,128)S(1)} %get-tuple-element.3) | data formatting | bytes 8388608

commit v3 on v2

--- a/solution.py
+++ b/solution.py
@@ -11,16 +11,18 @@
 gate_norm = 16.0
 LANES = 128
 SUBLANES = 8
-FF_SIZES = (1, 1, 2, 2, 2, 1)
+FF_SIZES = (1,)
 FF_Z = 2
-LAG_ZX = 7
+LAG_ZX = 8
 SQ_AT = 1
+A_SQ = 0
+A_SQZ = 0
+SQ_Z = 0
 A_ZF = 1
-LAG_ZACT = 11
-LAG_ACT = 9
-LAG_RELAY = 50
+LAG_ZACT = 12
+LAG_ACT = 11
 LAG_HAND = 100
-DIRECT = 99
+LAG_ZHAND = 100
 AX, AZ, BZ, BX, CY, DX, DZ, EZ, EX, FY, SQX, SQZ, ZF, XF, PHASES = 0, 1, 2, 3, 4, 5, 6, 7, 8, 9, 10, 12, 14, 16, 18
 F32 = jnp.float32
 BF16 = jnp.bfloat16
@@ -151,7 +153,6 @@
     fx_r,
     fz_r,
     hz_r,
-    hp_r,
     hx_r,
     zf_r,
 ):
@@ -334,7 +335,7 @@
             zf_send(0, px, zfr, lo, hi)
         else:
             send_x(AX, px, rx, ax_r.at[c], lo, hi)
-        if k == 1:
+        if k == A_SQ:
             squares_x(0, wide)
     load_decay = fetch(log_decay_hbm, log_decay_ref, in_sem.at[0])
     load_gain = fetch(out_gain_hbm, out_gain_ref, in_sem.at[1])
@@ -357,7 +358,7 @@
             zf_to_x(0, px, zfr, zfs, zfx, *bounds[a_zf])
         reduce_x(px, rx, pz, ax_r.at[c], lo, hi)
         send_z(AZ, pz, rz, az_r.at[c], lo, hi)
-        if k == 1:
+        if k == A_SQZ:
             squares_z(0)
 
     for d in range(1, n_in):
@@ -472,20 +473,12 @@
             squares_x(1, wide2)
 
     inv2 = [None]
-    half = n_out // 2
-
-    def relayed(c):
-        return n_out % 2 == 0 and c < n_c - DIRECT
-
-    def near_dev(d):
-        base = (zi // half) * half
-        return ((base + lax.rem(zi - base + d, half)) * n_in + xi, tp)
 
     def to_z(c):
         lo, hi = fbounds[c]
         reduce_x(fx, frx, fz, fx_r.at[c], lo, hi)
         send_z(DZ, fz, frz, fz_r.at[c], lo, hi)
-        if c == min(1, n_c - 2):
+        if c == SQ_Z:
             squares_z(1)
 
     def activate(c):
@@ -500,31 +493,19 @@
         cols = slice(*fchunks[c])
         hg[zi, xi, :, cols] = (jax.nn.silu(terms[:, :fc]) * terms[:, fc:]).astype(BF16)
         own = hg.at[zi, xi, :, cols]
-        if not relayed(c):
-            for d in range(1, n_out):
-                launch(EZ, own, own, hz_r.at[c], z_dev(d))
-            return
-        for d in range(1, half):
-            launch(EZ, own, own, hz_r.at[c], near_dev(d))
-        launch(EZ, own, own, hp_r.at[c], z_dev(half))
-
-    def relay(c):
-        if not relayed(c):
-            return
-        cols = slice(*fchunks[c])
-        slot = hg.at[z_peer(half), xi, :, cols]
-        took(slot, hp_r.at[c])
-        for d in range(1, half):
-            launch(EZ, slot, slot, hz_r.at[c], near_dev(d))
+        for d in range(1, n_out):
+            launch(EZ, own, own, hz_r.at[c], z_dev(d))
+        for d in range(1, n_in):
+            launch(EX, own, own, hx_r.at[c], x_dev(d))
 
     def hand_on(c):
         cols = slice(*fchunks[c])
-        far = 2 * (half - 1) if relayed(c) else n_out - 1
-        if far:
-            took(hg.at[:far, 0, :, cols], hz_r.at[c])
-        slot = hg.at[:, xi, :, cols]
+        if n_out > 1:
+            took(hg.at[: n_out - 1, 0, :, cols], hz_r.at[c])
         for d in range(1, n_in):
-            launch(EX, slot, slot, hx_r.at[c], x_dev(d))
+            for z in range(1, n_out):
+                slot = hg.at[z_back(z), xi, :, cols]
+                launch(EX, slot, slot, hx_r.at[c], x_dev(d))
 
     steps = []
     for c in range(n_c):
@@ -535,8 +516,7 @@
         else:
             steps.append((at, len(steps), to_z, c))
             steps.append((at + LAG_ACT, len(steps), activate, c))
-        steps.append((at + LAG_RELAY, len(steps), relay, c))
-        steps.append((at + LAG_HAND if c != d_zf else LAG_HAND, len(steps), hand_on, c))
+        steps.append((at + LAG_HAND if c != d_zf else LAG_ZHAND, len(steps), hand_on, c))
     for _, _, step, c in sorted(steps, key=lambda item: item[:2]):
         step(c)
 
@@ -632,7 +612,6 @@
         (n_a,),
         (1,),
         (4,),
-        (n_c,),
         (n_c,),
         (n_c,),
         (n_c,),

time: 54 us -> 51.9 us (0.961)
  Pallas kernels: 50.6 us -> 48.5 us
    pallas_call x1, Pallas kernels: 50.6 us -> 48.5 us  [body(): pl.pallas_call(functools.partial(kernel, n_kv, n_tp, feats * n_kv), out_s...]
where the time goes in v3:
time: 51.9 us; the launch traced here: 51.8 us
  Pallas kernels  48.5 us (93%)
  local copies, waits for them, and re-layouts  2.64 us (5%)
  between operations  0.64 us (1%)
    pallas_call x1, Pallas kernels, body(): pl.pallas_call(functools.partial(kernel, n_kv, n_tp, feats * n_kv), out_s...  48.5 us
    unnamed x2, local copies, waits for them, and re-layouts  2.64 us

profile of v3, /device:TPU:1, one launch (start us, length us, event | category | flops | bytes accessed | tf_op | source)
XLA Modules:
  0.0 51.8 jit_solution(7333460419307716701)
XLA Ops:
  0.6 48.5 %shard_map.158 = (bf16[128,256]{1,0:T(8,128)(2,1)S(1)}, f32[16,2,128,256]{3,2,1,0:T(8,128)S(1)}) custom-call(bf16[128,256]{1,0:T(8,128)(2,1)} %tokens_hbm.1, bf16[256]{0:T(256)(128)(2,1)} %norm_gain_hbm.1, bf16[256,256]{1,0:T(8,128)(2,1)} %wq_hbm.1, bf16[256,256]{1,0:T(8,128)(2,1)} %wk_hbm.1, bf16[256,512]{1,0:T(8,128)(2,1)} %wv_hbm.1, ...), custom_call_target="tpu_custom_call" | custom-call | tf_op jit(solution)/shard_map/pallas_call | solution.py:621
  49.1 0.6 %copy.19 = bf16[128,256]{1,0:T(8,128)(2,1)} copy(bf16[128,256]{1,0:T(8,128)(2,1)S(1)} %get-tuple-element.2) | data formatting | bytes 131072
  49.8 2.0 %copy.20 = f32[16,2,128,256]{3,2,1,0:T(8,128)} copy(f32[16,2,128,256]{3,2,1,0:T(8,128)S(1)} %get-tuple-element.3) | data formatting | bytes 8388608

commit v4 on v3

--- a/solution.py
+++ b/solution.py
@@ -13,6 +13,7 @@
 SUBLANES = 8
 FF_SIZES = (1,)
 FF_Z = 2
+FAR_FIRST = 1
 LAG_ZX = 8
 SQ_AT = 1
 A_SQ = 0
@@ -146,13 +147,10 @@
     bulk_sem,
     send_sem,
     sq_r,
-    ax_r,
-    az_r,
     mz_r,
     t_r,
     fx_r,
     fz_r,
-    hz_r,
     hx_r,
     zf_r,
 ):
@@ -185,6 +183,21 @@
 
     def t_dev(d):
         return (kv, lax.rem(tp + d, n_tp))
+
+    def z_targets():
+        if n_out % 2 or not FAR_FIRST:
+            return [(z_peer(d), d) for d in range(1, n_out)]
+        up = zi // (n_out // 2)
+        found = []
+        for j in range(n_out - 1):
+            high = n_out - 1 - j
+            from_top = high - 1 + (high - zi + n_out - 1) // n_out
+            from_bottom = j + 1 - (zi - j + n_out - 1) // n_out
+            target = up * from_bottom + (1 - up) * from_top
+            found.append((target, lax.rem(target - zi + n_out, n_out)))
+        return found
+
+    z_order = z_targets()
 
     def xt_dev(d, e):
         return (zi * n_in + x_peer(d), lax.rem(tp + e, n_tp))
@@ -242,13 +255,13 @@
             )
 
     def send_z(phase, src, dst, sem, lo, hi):
-        for d in range(1, n_out):
+        for z, d in z_order:
             launch(
                 phase,
-                src.at[z_peer(d), :, lo:hi],
+                src.at[z, :, lo:hi],
                 dst.at[d - 1, :, lo:hi],
                 sem,
-                z_dev(d),
+                (z * n_in + xi, tp),
             )
 
     def reduce_x(src, got, dst, sem, lo, hi):
@@ -268,8 +281,8 @@
         return total
 
     def zf_send(i, src, dst, lo, hi):
-        for d in range(1, n_out):
-            launch(ZF + i, src.at[:, z_peer(d), :, lo:hi], dst.at[d - 1], zf_r.at[i, 0], z_dev(d))
+        for z, d in z_order:
+            launch(ZF + i, src.at[:, z, :, lo:hi], dst.at[d - 1], zf_r.at[i, 0], (z * n_in + xi, tp))
 
     def zf_to_x(i, src, got, mid, dst, lo, hi):
         took(got, zf_r.at[i, 0])
@@ -306,8 +319,8 @@
         for d in range(1, n_in):
             total = total + sqx[i, d]
         sqz[i, 0] = total
-        for d in range(1, n_out):
-            launch(SQZ + i, sqz.at[i, 0], sqz.at[i, d], sq_r.at[i, 1], z_dev(d))
+        for z, d in z_order:
+            launch(SQZ + i, sqz.at[i, 0], sqz.at[i, d], sq_r.at[i, 1], (z * n_in + xi, tp))
 
     def inverse(i):
         if n_out > 1:
@@ -334,7 +347,7 @@
         if c == a_zf:
             zf_send(0, px, zfr, lo, hi)
         else:
-            send_x(AX, px, rx, ax_r.at[c], lo, hi)
+            send_x(AX, px, rx, fx_r.at[c], lo, hi)
         if k == A_SQ:
             squares_x(0, wide)
     load_decay = fetch(log_decay_hbm, log_decay_ref, in_sem.at[0])
@@ -356,8 +369,8 @@
         lo, hi = bounds[c]
         if a_zf is not None and k == len(x_order) - 1:
             zf_to_x(0, px, zfr, zfs, zfx, *bounds[a_zf])
-        reduce_x(px, rx, pz, ax_r.at[c], lo, hi)
-        send_z(AZ, pz, rz, az_r.at[c], lo, hi)
+        reduce_x(px, rx, pz, fx_r.at[c], lo, hi)
+        send_z(AZ, pz, rz, fz_r.at[c], lo, hi)
         if k == A_SQZ:
             squares_z(0)
 
@@ -367,7 +380,7 @@
     def arrived(c):
         if c == a_zf:
             return zf_final(0, zfs, zfx)
-        return reduce_z(pz, rz, az_r.at[c], *bounds[c])
+        return reduce_z(pz, rz, fz_r.at[c], *bounds[c])
 
 
     load_decay.wait()
@@ -397,7 +410,7 @@
 
     load_gain.wait()
     last = len(bounds) - 1
-    gate = reduce_z(pz, rz, az_r.at[last], *bounds[last]) * inv
+    gate = reduce_z(pz, rz, fz_r.at[last], *bounds[last]) * inv
     for h in range(heads):
         got = att[h]
         normed = (
@@ -409,8 +422,8 @@
         mg[zi, :, cols] = (normed * jax.nn.silu(gate[:, cols])).astype(BF16)
 
     own = mg.at[zi]
-    for d in range(1, n_out):
-        launch(BZ, own, own, mz_r.at[0], z_dev(d))
+    for z, _ in z_order:
+        launch(BZ, own, own, mz_r.at[0], (z * n_in + xi, tp))
     load_o.wait()
     if n_in > 1:
         took(wo.at[: n_in - 1], t_r.at[2])
@@ -493,15 +506,15 @@
         cols = slice(*fchunks[c])
         hg[zi, xi, :, cols] = (jax.nn.silu(terms[:, :fc]) * terms[:, fc:]).astype(BF16)
         own = hg.at[zi, xi, :, cols]
-        for d in range(1, n_out):
-            launch(EZ, own, own, hz_r.at[c], z_dev(d))
+        for z, _ in z_order:
+            launch(EZ, own, own, fx_r.at[c], (z * n_in + xi, tp))
         for d in range(1, n_in):
             launch(EX, own, own, hx_r.at[c], x_dev(d))
 
     def hand_on(c):
         cols = slice(*fchunks[c])
         if n_out > 1:
-            took(hg.at[: n_out - 1, 0, :, cols], hz_r.at[c])
+            took(hg.at[: n_out - 1, 0, :, cols], fx_r.at[c])
         for d in range(1, n_in):
             for z in range(1, n_out):
                 slot = hg.at[z_back(z), xi, :, cols]
@@ -608,13 +621,10 @@
         (4,),
         (PHASES,),
         (2, 2),
-        (n_a,),
-        (n_a,),
         (1,),
         (4,),
-        (n_c,),
-        (n_c,),
-        (n_c,),
+        (max(n_a, n_c),),
+        (max(n_a, n_c),),
         (n_c,),
         (2, 2),
     ]

time: 51.9 us -> 51.8 us (level)
  no operation moved by 1% of the time
where the time goes in v4:
time: 51.8 us; the launch traced here: 51.7 us
  Pallas kernels  48.4 us (93%)
  local copies, waits for them, and re-layouts  2.64 us (5%)
  between operations  0.64 us (1%)
    pallas_call x1, Pallas kernels, body(): pl.pallas_call(functools.partial(kernel, n_kv, n_tp, feats * n_kv), out_s...  48.4 us
    unnamed x2, local copies, waits for them, and re-layouts  2.64 us

profile of v4, /device:TPU:1, one launch (start us, length us, event | category | flops | bytes accessed | tf_op | source)
XLA Modules:
  0.0 51.7 jit_solution(9609075362717727697)
XLA Ops:
  0.6 48.4 %shard_map.158 = (bf16[128,256]{1,0:T(8,128)(2,1)S(1)}, f32[16,2,128,256]{3,2,1,0:T(8,128)S(1)}) custom-call(bf16[128,256]{1,0:T(8,128)(2,1)} %tokens_hbm.1, bf16[256]{0:T(256)(128)(2,1)} %norm_gain_hbm.1, bf16[256,256]{1,0:T(8,128)(2,1)} %wq_hbm.1, bf16[256,256]{1,0:T(8,128)(2,1)} %wk_hbm.1, bf16[256,512]{1,0:T(8,128)(2,1)} %wv_hbm.1, ...), custom_call_target="tpu_custom_call" | custom-call | tf_op jit(solution)/shard_map/pallas_call | solution.py:631
  49.0 0.6 %copy.19 = bf16[128,256]{1,0:T(8,128)(2,1)} copy(bf16[128,256]{1,0:T(8,128)(2,1)S(1)} %get-tuple-element.2) | data formatting | bytes 131072
  49.7 2.0 %copy.20 = f32[16,2,128,256]{3,2,1,0:T(8,128)} copy(f32[16,2,128,256]{3,2,1,0:T(8,128)S(1)} %get-tuple-element.3) | data formatting | bytes 8388608

commit v5 on v4

--- a/solution.py
+++ b/solution.py
@@ -14,6 +14,7 @@
 FF_SIZES = (1,)
 FF_Z = 2
 FAR_FIRST = 1
+DIRECT = 2
 LAG_ZX = 8
 SQ_AT = 1
 A_SQ = 0
@@ -510,11 +511,19 @@
             launch(EZ, own, own, fx_r.at[c], (z * n_in + xi, tp))
         for d in range(1, n_in):
             launch(EX, own, own, hx_r.at[c], x_dev(d))
+            if direct(c):
+                for z, _ in z_order:
+                    launch(EX, own, own, hx_r.at[c], (z * n_in + x_peer(d), tp))
+
+    def direct(c):
+        return n_c - 1 - DIRECT <= c < n_c - 1
 
     def hand_on(c):
         cols = slice(*fchunks[c])
         if n_out > 1:
             took(hg.at[: n_out - 1, 0, :, cols], fx_r.at[c])
+        if direct(c):
+            return
         for d in range(1, n_in):
             for z in range(1, n_out):
                 slot = hg.at[z_back(z), xi, :, cols]

time: 51.8 us -> 51.8 us (level)
  no operation moved by 1% of the time
where the time goes in v5:
time: 51.8 us; the launch traced here: 51.6 us
  Pallas kernels  48.3 us (93%)
  local copies, waits for them, and re-layouts  2.64 us (5%)
  between operations  0.64 us (1%)
    pallas_call x1, Pallas kernels, body(): pl.pallas_call(functools.partial(kernel, n_kv, n_tp, feats * n_kv), out_s...  48.3 us
    unnamed x2, local copies, waits for them, and re-layouts  2.64 us

profile of v5, /device:TPU:1, one launch (start us, length us, event | category | flops | bytes accessed | tf_op | source)
XLA Modules:
  0.0 51.6 jit_solution(1264687458196514035)
XLA Ops:
  0.6 48.3 %shard_map.158 = (bf16[128,256]{1,0:T(8,128)(2,1)S(1)}, f32[16,2,128,256]{3,2,1,0:T(8,128)S(1)}) custom-call(bf16[128,256]{1,0:T(8,128)(2,1)} %tokens_hbm.1, bf16[256]{0:T(256)(128)(2,1)} %norm_gain_hbm.1, bf16[256,256]{1,0:T(8,128)(2,1)} %wq_hbm.1, bf16[256,256]{1,0:T(8,128)(2,1)} %wk_hbm.1, bf16[256,512]{1,0:T(8,128)(2,1)} %wv_hbm.1, ...), custom_call_target="tpu_custom_call" | custom-call | tf_op jit(solution)/shard_map/pallas_call | solution.py:640
  49.0 0.6 %copy.19 = bf16[128,256]{1,0:T(8,128)(2,1)} copy(bf16[128,256]{1,0:T(8,128)(2,1)S(1)} %get-tuple-element.2) | data formatting | bytes 131072
  49.6 2.0 %copy.20 = f32[16,2,128,256]{3,2,1,0:T(8,128)} copy(f32[16,2,128,256]{3,2,1,0:T(8,128)S(1)} %get-tuple-element.3) | data formatting | bytes 8388608
